TPU v7x, 32 devices: a whole 2x2x4 slice. The times are simulated.
32 devices in a mesh: sp: 4 (over y, x), tp: 8 (over z, core).
Axes of the slice: x: 2, y: 2, z: 4, core: 2. Of those that a mesh axis runs over, the one named last changes fastest.
Arguments:
- queries: bfloat16 [1536, 2048], P('sp', 'tp'), may hold values from -6 to 6
- cell_key_rows: bfloat16 [1536, 2048], P('sp', 'tp'), may hold values from -6 to 6
- cell_value_rows: bfloat16 [1536, 2048], P('sp', 'tp'), may hold values from -6 to 6
- output_gate_logits: bfloat16 [1536, 2048], P('sp', 'tp'), may hold values from -6 to 6
- input_gate_logs: float32 [16, 1536], P('tp', 'sp'), may hold values from -5 to 250
- forget_gate_logits: float32 [16, 1536], P('tp', 'sp'), may hold values from 1 to 13
- extra_log_forget: float32 [16, 1536], P('tp', 'sp'), may hold values from -0.7 to 0
- head_norm_gain: float32 [2048], P('tp'), may hold values from 0.1 to 1.9
- cell_output_matrix: bfloat16 [2048, 4096], P('tp'), may hold values from -0.125 to 0.125
- residual: bfloat16 [1536, 4096], P('sp'), may hold values from -6 to 6
- expert_norm_gain: float32 [4096], replicated, may hold values from 0.1 to 1.9
- routes: int32 [1536, 2], P('sp'), may hold values from 0 to 3, all different within a row; in each aligned block of 48 rows (0 to 47, 48 to 95, ...) at most 48 rows name the same one
- token_expert_weights: float32 [1536, 2], P('sp'), may hold values from 0.2 to 1
- expert_gate_matrix: bfloat16 [4, 4096, 2048], P('sp', None, 'tp'), may hold values from -0.09375 to 0.09375
- expert_up_matrix: bfloat16 [4, 4096, 2048], P('sp', None, 'tp'), may hold values from -0.09375 to 0.09375
- expert_down_matrix: bfloat16 [4, 2048, 4096], P('sp', 'tp'), may hold values from -0.125 to 0.125
Outputs:
- layer_out: bfloat16 [1536, 4096], P(('sp', 'tp'))
Inputs may be any that keep to these rules, and one draw needn't show every extreme that they name: `routes`: each row names 2 different experts. In the rows of one device (aligned blocks of 48 rows) no expert is named more than 48 times, and in some blocks one expert is named exactly 48 times.
All inputs are finite; a program needn't handle non-finite values.
Results may differ from a plain program's by a relative error of at most 0.019.
Values may be sent and summed in bfloat16 or wider, within the bound.
A program may use at most 128 MiB of HBM per device.

v0:
```python
import jax
import jax.numpy as jnp
from jax import lax
from jax.sharding import PartitionSpec as P

HEAD_DIM = 128
BLOCK = 128
floor_neg = -1e30
norm_eps = 1e-06


def entering(x, axis, combine, identity):
    count, here = (lax.axis_size(axis), lax.axis_index(axis))
    everything = jax.tree.map(lambda part: lax.all_gather(part, axis), x)
    start = jax.tree.map(
        lambda part, zero: jnp.broadcast_to(jnp.asarray(zero, part.dtype), part.shape), x, identity
    )

    def lap(k, before):
        reached = k < here
        new = combine(before, jax.tree.map(lambda part: part[k], everything))
        return jax.tree.map(lambda a, b: jnp.where(reached, a, b), new, before)

    return lax.fori_loop(0, count, lap, start)


def block_cells(query_f, key_f, value_f, input_f, forget_log_values, start_cell, start_stab):
    heads, length, width = query_f.shape
    count = length // BLOCK
    highest = lax.Precision.HIGHEST

    def split(array):
        return jnp.moveaxis(array.reshape((heads, count, BLOCK) + array.shape[2:]), 1, 0)

    causal = jnp.tril(jnp.ones((BLOCK, BLOCK), dtype=bool))

    def advance(carry, block):
        cell, stab = carry
        qblock, kblock, vblock, iblock, fblock = block
        cumul = jnp.cumsum(fblock, axis=-1)
        total = cumul[:, -1]
        log_inner = jnp.where(
            causal[None], cumul[:, :, None] - cumul[:, None, :] + iblock[:, None, :], floor_neg
        )
        carried = cumul + stab[:, None]
        stab_row = jnp.maximum(carried, jnp.max(log_inner, axis=-1))
        scores = jnp.einsum("hld,hsd->hls", qblock, kblock, precision=highest) * jnp.exp(
            log_inner - stab_row[..., None]
        )
        numer = jnp.einsum("hls,hsd->hld", scores, vblock, precision=highest) + jnp.exp(
            carried - stab_row
        )[..., None] * jnp.einsum("hld,hde->hle", qblock, cell, precision=highest)
        log_write = total[:, None] - cumul + iblock
        stab_next = jnp.maximum(total + stab, jnp.max(log_write, axis=-1))
        weights = jnp.exp(log_write - stab_next[:, None])
        cell_next = jnp.exp(total + stab - stab_next)[:, None, None] * cell + jnp.einsum(
            "hsd,hse->hde", kblock * weights[..., None], vblock, precision=highest
        )
        return ((cell_next, stab_next), (numer, stab_row))

    inputs = tuple(
        (split(array) for array in (query_f, key_f, value_f, input_f, forget_log_values))
    )
    unused, (numer, stab_rows) = lax.scan(advance, (start_cell, start_stab), inputs)
    numer = jnp.moveaxis(numer, 0, 1).reshape(heads, length, width)
    stab_rows = jnp.moveaxis(stab_rows, 0, 1).reshape(heads, length)
    return (numer, stab_rows)


def combine_states(earlier, later):
    cell_early, stab_early, total_early = earlier
    cell_late, stab_late, total_late = later
    stab = jnp.maximum(total_late + stab_early, stab_late)
    cell = (
        jnp.exp(total_late + stab_early - stab)[:, None, None] * cell_early
        + jnp.exp(stab_late - stab)[:, None, None] * cell_late
    )
    return (cell, stab, total_early + total_late)


def rms_scale(rows, gain):
    values = rows.astype(jnp.float32)
    return (
        values * lax.rsqrt(jnp.mean(values * values, axis=-1, keepdims=True) + norm_eps) * gain
    ).astype(jnp.bfloat16)


def slot_tables(block_routes, experts, capacity):
    flat = block_routes.reshape(-1)
    count = flat.shape[0]
    topk = block_routes.shape[1]
    onehot = (flat[:, None] == jnp.arange(experts, dtype=jnp.int32)[None, :]).astype(jnp.int32)
    before = jnp.cumsum(onehot, axis=0) - onehot
    position = jnp.sum(before * onehot, axis=1)
    slot = flat * capacity + position
    match = slot[None, :] == jnp.arange(experts * capacity, dtype=jnp.int32)[:, None]
    owner = jnp.arange(count, dtype=jnp.int32)[None, :] // topk + 1
    source = jnp.sum(jnp.where(match, owner, 0), axis=1) - 1
    return (slot, source)


def fill_slots(rows, source):
    picked = rows[jnp.maximum(source, 0)]
    return jnp.where((source >= 0)[:, None], picked, jnp.zeros_like(picked))


def local(
    queries,
    cell_key_rows,
    cell_value_rows,
    output_gate_logits,
    input_gate_logs,
    forget_gate_logits,
    extra_log_forget,
    head_norm_gain,
    cell_output_matrix,
    residual,
    expert_norm_gain,
    routes,
    token_expert_weights,
    expert_gate_matrix,
    expert_up_matrix,
    expert_down_matrix,
):
    length = queries.shape[0]
    heads = queries.shape[1] // HEAD_DIM
    tp_count = lax.axis_size("tp")
    experts = lax.axis_size("sp")
    topk = routes.shape[1]
    tokens = length // tp_count
    capacity = max(2, 2 * tokens * topk // experts)
    highest = lax.Precision.HIGHEST
    tp_index = lax.axis_index("tp")

    def heads_of(array):
        return jnp.transpose(array.astype(jnp.float32).reshape(length, heads, HEAD_DIM), (1, 0, 2))

    query_f = heads_of(queries)
    key_f = heads_of(cell_key_rows) * HEAD_DIM ** (-0.5)
    value_f = heads_of(cell_value_rows)
    forget_log_values = jax.nn.log_sigmoid(forget_gate_logits) + extra_log_forget
    running = jnp.cumsum(forget_log_values, axis=1)
    total_dev = running[:, -1]
    log_write = input_gate_logs + total_dev[:, None] - running
    stab_dev = jnp.max(log_write, axis=1)
    cell_dev = jnp.einsum(
        "hsd,hse->hde",
        key_f * jnp.exp(log_write - stab_dev[:, None])[..., None],
        value_f,
        precision=highest,
    )
    identity = (
        jnp.zeros_like(cell_dev),
        jnp.full_like(stab_dev, floor_neg),
        jnp.zeros_like(total_dev),
    )
    prefix_cell, prefix_stab, prefix_total = entering(
        (cell_dev, stab_dev, total_dev), "sp", combine_states, identity
    )
    start_stab = jnp.maximum(prefix_stab, prefix_total)
    start_cell = jnp.exp(prefix_stab - start_stab)[:, None, None] * prefix_cell
    numer = block_cells(
        query_f, key_f, value_f, input_gate_logs, forget_log_values, start_cell, start_stab
    )[0]
    scaled = (
        numer
        * lax.rsqrt(jnp.mean(numer * numer, axis=2, keepdims=True) + norm_eps)
        * head_norm_gain.reshape(heads, 1, HEAD_DIM)
    )
    mixed = jnp.transpose(scaled, (1, 0, 2)).reshape(length, heads * HEAD_DIM)
    cell_out = (jax.nn.sigmoid(output_gate_logits.astype(jnp.float32)) * mixed).astype(jnp.bfloat16)
    gate_local = expert_gate_matrix[0]
    up_local = expert_up_matrix[0]
    down_local = expert_down_matrix[0]
    projected = lax.psum_scatter(
        jnp.dot(cell_out, cell_output_matrix, preferred_element_type=jnp.float32).astype(
            jnp.bfloat16
        ),
        "tp",
        scatter_dimension=0,
        tiled=True,
    ).astype(jnp.float32)
    own_residual = lax.dynamic_slice_in_dim(residual, tp_index * tokens, tokens, 0)
    after_mix = (own_residual.astype(jnp.float32) + projected).astype(jnp.bfloat16)
    own_routes = lax.dynamic_slice_in_dim(routes, tp_index * tokens, tokens, 0)
    slot, source = slot_tables(own_routes, experts, capacity)
    moe_in = rms_scale(after_mix, expert_norm_gain)
    sent = fill_slots(moe_in, source).reshape(experts, capacity, moe_in.shape[1])
    arrived = lax.all_to_all(sent, "sp", split_axis=0, concat_axis=0, tiled=True)
    piece = lax.all_gather(arrived, "tp", axis=0, tiled=True)
    gate = jnp.einsum("rcd,df->rcf", piece, gate_local, preferred_element_type=jnp.float32)
    upper = jnp.einsum("rcd,df->rcf", piece, up_local, preferred_element_type=jnp.float32)
    hidden = (jax.nn.silu(gate) * upper).astype(jnp.bfloat16)
    summed = lax.psum_scatter(
        jnp.einsum("rcf,fd->rcd", hidden, down_local, preferred_element_type=jnp.float32).astype(
            jnp.bfloat16
        ),
        "tp",
        scatter_dimension=0,
        tiled=True,
    )
    returned = lax.all_to_all(summed, "sp", split_axis=0, concat_axis=0, tiled=True)
    width = returned.shape[2]
    chosen = returned.reshape(experts * capacity, width)[slot].reshape(tokens, topk, width)
    own_weight = lax.dynamic_slice_in_dim(token_expert_weights, tp_index * tokens, tokens, 0)
    moe = jnp.sum(own_weight[:, :, None] * chosen.astype(jnp.float32), axis=1)
    return (after_mix.astype(jnp.float32) + moe).astype(jnp.bfloat16)


def solution(mesh):
    placed = (
        P("sp", "tp"),
        P("sp", "tp"),
        P("sp", "tp"),
        P("sp", "tp"),
        P("tp", "sp"),
        P("tp", "sp"),
        P("tp", "sp"),
        P("tp"),
        P("tp", None),
        P("sp", None),
        P(),
        P("sp", None),
        P("sp", None),
        P("sp", None, "tp"),
        P("sp", None, "tp"),
        P("sp", "tp", None),
    )
    return jax.shard_map(
        local, mesh=mesh, in_specs=placed, out_specs=P(("sp", "tp"), None), check_vma=False
    )
```

profile of v0, /device:TPU:0, one launch (start us, length us, event | category | flops | bytes accessed | tf_op | source)
XLA Modules:
  0.0 442.5 jit_solution(5801461110125140041)
XLA Ops:
  6.5 0.9 fusion.70
  9.4 0.9 fusion.61
  10.3 1.3 dynamic-slice
  12.7 11.4 %all-reduce.2 = (f32[8]{0:T(128)S(1)}, f32[8]{0:T(128)S(1)}) all-reduce(f32[8]{0:T(128)S(1)} %dynamic-update-slice, f32[8]{0:T(128)S(1)} %dynamic-update-slice.1), channel_id=2, replica_groups=mesh['sp'=4,'tp'=8] {'sp'}, use_global_device_ids=true, to_apply=%add | all-reduce | flops 16 | bytes 128
  24.9 1.1 copy.71
  26.0 1.1 copy.72
  27.7 9.8 %all-gather.2 = f32[8,128,128]{2,1,0:T(8,128)S(1)} all-gather(f32[2,128,128]{2,1,0:T(8,128)S(1)} %fusion.49), channel_id=4, replica_groups=mesh['sp'=4,'tp'=8] {'sp'}, dimensions={0}, use_global_device_ids=true | all-gather | bytes 655360 | tf_op jit(solution)/shard_map/all_gather | solution.py:14
  37.5 3.3 while.34
  41.0 1.1 copy.76
  42.8 1.1 copy.77
  44.1 11.7 %while.33 = (s32[]{:T(128)}, f32[2,128,128]{2,1,0:T(8,128)S(1)}, f32[2]{0:T(128)S(1)}, f32[3,2,128,128]{3,2,0,1:T(8,128)}, f32[3,2,128]{2,1,0:T(2,128)S(1)}, /*i...) while((s32[]{:T(128)}, f32[2,128,128]{2,1,0:T(8,128)S(1)}, ...), condition=%wide.region_9.10_spmd.clone, body=%wide.region_5.9_spmd.clone.sunk | while | flops 201835776 | bytes 1911509 | solution.py:64
  46.5 0.9 fusion.95
  48.5 0.9 fusion.92
  50.4 0.9 fusion.95
  54.2 0.9 fusion.95
  55.8 1.2 fusion.46
  57.0 1.2 fusion.44
  58.7 4.3 convolution_convert_fusion.1
  64.7 39.1 %reduce-scatter.3.cloned.1.call-done = bf16[48,4096]{1,0:T(8,128)(2,1)} async-done(((bf16[384,4096]{1,0:T(8,128)(2,1)}), bf16[48,4096]{1,0:T(8,128)(2,1)}) %reduce-scatter.3.cloned.1.call-update) | async-done | bytes 393232 | tf_op jit(solution)/shard_map/reduce_scatter | solution.py:175
  103.8 1.4 fusion.39
  105.4 2.7 gather_fusion
  108.0 1.6 broadcast_select_fusion.4
  109.6 21.1 %all_to_all.10 = bf16[4,48,4096]{2,1,0:T(8,128)(2,1)} all-to-all(bf16[4,48,4096]{2,1,0:T(8,128)(2,1)S(1)} %broadcast_select_fusion.4), channel_id=1, replica_groups=mesh['sp'=4,'tp'=8] {'sp'}, dimensions={0} | all-to-all | bytes 3145728 | tf_op jit(solution)/shard_map/all_to_all | solution.py:189
  131.0 116.1 %all-gather.5.cloned.1.call-done = bf16[32,48,4096]{2,1,0:T(8,128)(2,1)} async-done(((bf16[4,48,4096]{2,1,0:T(8,128)(2,1)}), bf16[32,48,4096]{2,1,0:T(8,128)(2,1)}) %all-gather.5.cloned.1.call-update) | async-done | bytes 12582928 | tf_op jit(solution)/shard_map/all_gather | solution.py:190
  247.1 9.9 %fusion.33 = f32[32,48,256]{2,1,0:T(8,128)} fusion(bf16[32,48,4096]{2,1,0:T(8,128)(2,1)} %all-gather.5.cloned.1.call-done, bf16[1,4096,256]{2,1,0:T(8,128)(2,1)} %param.33), kind=kOutput, calls=%fused_computation.59 | convolution fusion | flops 3221225472 | bytes 16252928 | tf_op jit(solution)/shard_map/rcd,df->rcf/dot_general | solution.py:191
  257.0 19.4 %convolution_convert_fusion = bf16[32,48,4096]{2,1,0:T(8,128)(2,1)} fusion(bf16[1,256,4096]{2,1,0:T(8,128)(2,1)S(1)} %copy-done, f32[32,48,256]{2,1,0:T(8,128)} %fusion.33, bf16[32,48,4096]{2,1,0:T(8,128)(2,1)} %all-gather.5.cloned.1.call-done, bf16[1,4096,256]{2,1,0:T(8,128)(2,1)} %param.34), kind=kOutput, calls=%fused_computation.54 | convolution fusion | flops 6451101696 | bytes 30932992 | tf_op jit(solution)/shard_map/rcf,fd->rcd/dot_general | solution.py:195
  276.4 127.5 %reduce-scatter.5.cloned.1.call-done = bf16[4,48,4096]{2,1,0:T(8,128)(2,1)} async-done(((bf16[32,48,4096]{2,1,0:T(8,128)(2,1)}), bf16[4,48,4096]{2,1,0:T(8,128)(2,1)}) %reduce-scatter.5.cloned.1.call-update) | async-done | bytes 1572880 | tf_op jit(solution)/shard_map/reduce_scatter | solution.py:194
  403.9 4.6 %all-to-all-start.1 = ((bf16[4,48,4096]{2,1,0:T(8,128)(2,1)}), bf16[4,48,4096]{2,1,0:T(8,128)(2,1)}, u32[]{:S(2)}, u32[]{:S(2)}) async-start(bf16[4,48,4096]{2,1,0:T(8,128)(2,1)} %reduce-scatter.5.cloned.1.call-done), calls=%async_computation.3 | async-start | bytes 3145728 | tf_op jit(solution)/shard_map/all_to_all | solution.py:202
  409.6 16.4 %all-to-all-done.1 = bf16[4,48,4096]{2,1,0:T(8,128)(2,1)} async-done(((bf16[4,48,4096]{2,1,0:T(8,128)(2,1)}), bf16[4,48,4096]{2,1,0:T(8,128)(2,1)}, u32[]{:S(2)}, u32[]{:S(2)}) %all-to-all-start.1) | async-done | bytes 1572896 | tf_op jit(solution)/shard_map/all_to_all | solution.py:202
  426.0 3.4 gather_fusion.1
  429.4 2.1 reshape.291
  431.5 3.6 multiply_reduce_fusion
  (113 shorter events, 20.3 us)
Async XLA Ops:
  6.5 250.4 %copy-start = (bf16[1,256,4096]{2,1,0:T(8,128)(2,1)S(1)}, bf16[1,256,4096]{2,1,0:T(8,128)(2,1)}, u32[]{:S(2)}) copy-start(bf16[1,256,4096]{2,1,0:T(8,128)(2,1)} %param.35) | copy-start | bytes 6291460
  6.5 97.3 %reduce-scatter.3.cloned.1.call-start = ((), (), s32[]{:S(2)}) async-start(), calls=%async_computation.4 | async-start | bytes 3538944 | tf_op jit(solution)/shard_map/reduce_scatter | solution.py:175
  44.1 12.9 %copy-start.3 = (f32[256]{0:T(256)S(1)}, f32[256]{0:T(256)}, u32[]{:S(2)}) copy-start(f32[256]{0:T(256)} %param.27) | copy-start | bytes 3076
  55.8 2.6 copy-start.1
  63.0 42.2 %copy-start.2 = (f32[4096]{0:T(1024)S(1)}, f32[4096]{0:T(1024)}, u32[]{:S(2)}) copy-start(f32[4096]{0:T(1024)} %param.30) | copy-start | bytes 49156
  63.0 184.1 %all-gather.5.cloned.1.call-start = ((), (), s32[]{:S(2)}) async-start(), calls=%async_computation.5 | async-start | bytes 14155776 | tf_op jit(solution)/shard_map/all_gather | solution.py:190
  130.8 273.1 %reduce-scatter.5.cloned.1.call-start = ((), (), s32[]{:S(2)}) async-start(), calls=%async_computation.6 | async-start | bytes 14155776 | tf_op jit(solution)/shard_map/reduce_scatter | solution.py:194
  403.9 22.1 %all-to-all-start.1 = ((bf16[4,48,4096]{2,1,0:T(8,128)(2,1)}), bf16[4,48,4096]{2,1,0:T(8,128)(2,1)}, u32[]{:S(2)}, u32[]{:S(2)}) async-start(bf16[4,48,4096]{2,1,0:T(8,128)(2,1)} %reduce-scatter.5.cloned.1.call-done), calls=%async_computation.3 | async-start | bytes 3145728 | tf_op jit(solution)/shard_map/all_to_all | solution.py:202
Sparse Core Ops, SparseCore 0:
  63.1 40.6 reduce-scatter.2
  130.9 116.1 all-gather.4
  276.5 127.3 reduce-scatter.4
where the time goes:
time: 443 us; the launch traced here: 442 us
  waiting for transfers between devices  299 us (67%)
  blocking collectives  42.3 us (10%)
  matrix products  40.3 us (9%)
  other arithmetic  23.5 us (5%)
  local copies, waits for them, and re-layouts  18.1 us (4%)
  between operations  14.1 us (3%)
  starting transfers between devices  4.82 us (1%)
    reduce_scatter x1, waiting for transfers between devices, local(): lax.psum_scatter(jnp.einsum('rcf,fd->rcd', hidden, down_local, preferred_...  127 us
    all_gather x1, waiting for transfers between devices, local(): piece = lax.all_gather(arrived, 'tp', axis=0, tiled=True)  116 us
    reduce_scatter x1, waiting for transfers between devices, local(): lax.psum_scatter(jnp.dot(cell_out, cell_output_matrix, preferred_element_...  39.1 us
    all_to_all x1, blocking collectives, local(): lax.all_to_all(sent, 'sp', split_axis=0, concat_axis=0, tiled=True)  21.1 us
    dot_general x1, matrix products, local(): jnp.einsum('rcf,fd->rcd', hidden, down_local, preferred_element_type=jnp....  19.4 us
    all_to_all x1, waiting for transfers between devices, local(): lax.all_to_all(summed, 'sp', split_axis=0, concat_axis=0, tiled=True)  16.4 us
    unnamed x1, blocking collectives  11.4 us
    dot_general x1, matrix products, local(): jnp.einsum('rcd,df->rcf', piece, gate_local, preferred_element_type=jnp.f...  9.86 us
  transfers between devices with their start and end apart: 4, of which 4 were waited for; matrix products, arithmetic and copies ran while one was open for 1% of the time, Pallas kernels for 0%

commit v1 on v0

--- a/solution.py
+++ b/solution.py
@@ -1,3 +1,4 @@
+import functools
 import jax
 import jax.numpy as jnp
 from jax import lax
@@ -7,6 +8,22 @@
 BLOCK = 128
 floor_neg = -1e30
 norm_eps = 1e-06
+
+
+def paths_wait(u_in, along_dim):
+    count_all = lax.psum(1, axis_name="tp")
+    view_out = u_in
+    v1 = sorted(((dd, (dd + 1) % count_all) for dd in range(count_all)))
+    slots = [view_out]
+    for nth in range(1, count_all):
+        view_out = lax.ppermute(view_out, axis_name="tp", perm=v1)
+        slots.insert(0, view_out)
+    u1 = jnp.concatenate(slots, axis=along_dim)
+    built = lax.axis_index("tp") + 1
+    return jnp.roll(u1, built * u_in.shape[along_dim], axis=along_dim)
+
+
+save_ends_on_mesh = functools.partial(paths_wait, along_dim=0)
 
 
 def entering(x, axis, combine, identity):
@@ -187,7 +204,7 @@
     moe_in = rms_scale(after_mix, expert_norm_gain)
     sent = fill_slots(moe_in, source).reshape(experts, capacity, moe_in.shape[1])
     arrived = lax.all_to_all(sent, "sp", split_axis=0, concat_axis=0, tiled=True)
-    piece = lax.all_gather(arrived, "tp", axis=0, tiled=True)
+    piece = save_ends_on_mesh(arrived)
     gate = jnp.einsum("rcd,df->rcf", piece, gate_local, preferred_element_type=jnp.float32)
     upper = jnp.einsum("rcd,df->rcf", piece, up_local, preferred_element_type=jnp.float32)
     hidden = (jax.nn.silu(gate) * upper).astype(jnp.bfloat16)

time: 443 us -> 513 us (1.16)
  local copies, waits for them, and re-layouts: 18.1 us -> 55.7 us
  waiting for transfers between devices: 299 us -> 333 us
    ppermute x0 -> x7, waiting for transfers between devices: none -> 152 us  [paths_wait(): view_out = lax.ppermute(view_out, axis_name='tp', perm=v1)]
    all_gather x1 -> x0, waiting for transfers between devices: 116 us -> none  [local(): piece = lax.all_gather(arrived, 'tp', axis=0, tiled=True)]
    unnamed x19 -> x60, local copies, waits for them, and re-layouts: 5.24 us -> 41.6 us
  transfers between devices with their start and end apart: 4 -> 10, of which waited for: 4 -> 10; matrix products, arithmetic and copies ran while one was open for 1% -> 1% of each run, Pallas kernels for 0% -> 0%
where the time goes in v1:
time: 513 us; the launch traced here: 512 us
  waiting for transfers between devices  333 us (65%)
  local copies, waits for them, and re-layouts  55.7 us (11%)
  blocking collectives  42.2 us (8%)
  matrix products  38.1 us (7%)
  other arithmetic  23.5 us (5%)
  between operations  14.4 us (3%)
    ppermute x7, waiting for transfers between devices, paths_wait(): view_out = lax.ppermute(view_out, axis_name='tp', perm=v1)  152 us
    reduce_scatter x1, waiting for transfers between devices, local(): lax.psum_scatter(jnp.einsum('rcf,fd->rcd', hidden, down_local, preferred_...  126 us
    unnamed x60, local copies, waits for them, and re-layouts  41.6 us
    reduce_scatter x1, waiting for transfers between devices, local(): lax.psum_scatter(jnp.dot(cell_out, cell_output_matrix, preferred_element_...  39.1 us
    all_to_all x1, blocking collectives, local(): lax.all_to_all(sent, 'sp', split_axis=0, concat_axis=0, tiled=True)  21 us
    dot_general x1, matrix products, local(): jnp.einsum('rcf,fd->rcd', hidden, down_local, preferred_element_type=jnp....  19.6 us
    all_to_all x1, waiting for transfers between devices, local(): lax.all_to_all(summed, 'sp', split_axis=0, concat_axis=0, tiled=True)  16.4 us
    unnamed x1, blocking collectives  11.4 us
  transfers between devices with their start and end apart: 10, of which 10 were waited for; matrix products, arithmetic and copies ran while one was open for 1% of the time, Pallas kernels for 0%

profile of v1, /device:TPU:0, one launch (start us, length us, event | category | flops | bytes accessed | tf_op | source)
XLA Modules:
  0.0 512.2 jit_solution(7033482047093833994)
XLA Ops:
  10.3 1.3 dynamic-slice
  12.7 11.4 %all-reduce.2 = (f32[8]{0:T(128)S(1)}, f32[8]{0:T(128)S(1)}) all-reduce(f32[8]{0:T(128)S(1)} %dynamic-update-slice, f32[8]{0:T(128)S(1)} %dynamic-update-slice.1), channel_id=2, replica_groups=mesh['sp'=4,'tp'=8] {'sp'}, use_global_device_ids=true, to_apply=%add | all-reduce | flops 16 | bytes 128
  27.7 9.8 %all-gather.2 = f32[8,128,128]{2,1,0:T(8,128)S(1)} all-gather(f32[2,128,128]{2,1,0:T(8,128)S(1)} %fusion.47), channel_id=4, replica_groups=mesh['sp'=4,'tp'=8] {'sp'}, dimensions={0}, use_global_device_ids=true | all-gather | bytes 655360 | tf_op jit(solution)/shard_map/all_gather | solution.py:31
  37.5 3.3 while.34
  44.1 11.7 %while.33 = (s32[]{:T(128)}, f32[2,128,128]{2,1,0:T(8,128)S(1)}, f32[2]{0:T(128)S(1)}, f32[3,2,128,128]{3,2,0,1:T(8,128)}, f32[3,2,128]{2,1,0:T(2,128)S(1)}, /*i...) while((s32[]{:T(128)}, f32[2,128,128]{2,1,0:T(8,128)S(1)}, ...), condition=%wide.region_9.10_spmd.clone, body=%wide.region_5.9_spmd.clone.sunk | while | flops 201835776 | bytes 1911509 | solution.py:81
  58.7 4.3 convolution_convert_fusion.1
  64.7 39.1 %reduce-scatter.3.cloned.1.call-done = bf16[48,4096]{1,0:T(8,128)(2,1)} async-done(((bf16[384,4096]{1,0:T(8,128)(2,1)}), bf16[48,4096]{1,0:T(8,128)(2,1)}) %reduce-scatter.3.cloned.1.call-update) | async-done | bytes 393232 | tf_op jit(solution)/shard_map/reduce_scatter | solution.py:192
  103.8 1.4 fusion.37
  105.4 2.7 gather_fusion
  108.0 1.6 broadcast_select_fusion.4
  109.6 21.0 %all_to_all.10 = bf16[4,48,4096]{2,1,0:T(8,128)(2,1)S(1)} all-to-all(bf16[4,48,4096]{2,1,0:T(8,128)(2,1)S(1)} %broadcast_select_fusion.4), channel_id=1, replica_groups=mesh['sp'=4,'tp'=8] {'sp'}, dimensions={0} | all-to-all | bytes 3145728 | tf_op jit(solution)/shard_map/all_to_all | solution.py:206
  131.8 21.6 %collective-permute-done = bf16[4,48,4096]{2,1,0:T(8,128)(2,1)S(1)} collective-permute-done((bf16[4,48,4096]{2,1,0:T(8,128)(2,1)S(1)}, bf16[4,48,4096]{2,1,0:T(8,128)(2,1)S(1)}, u32[]{:S(2)}, u32[]{:S(2)}) %collective-permute-start) | collective-permute-done | bytes 1572896 | tf_op jit(solution)/shard_map/ppermute | solution.py:19
  154.6 21.6 %collective-permute-done.1 = bf16[4,48,4096]{2,1,0:T(8,128)(2,1)S(1)} collective-permute-done((bf16[4,48,4096]{2,1,0:T(8,128)(2,1)S(1)}, bf16[4,48,4096]{2,1,0:T(8,128)(2,1)S(1)}, u32[]{:S(2)}, u32[]{:S(2)}) %collective-permute-start.1) | collective-permute-done | bytes 1572896 | tf_op jit(solution)/shard_map/ppermute | solution.py:19
  177.4 21.6 %collective-permute-done.2 = bf16[4,48,4096]{2,1,0:T(8,128)(2,1)S(1)} collective-permute-done((bf16[4,48,4096]{2,1,0:T(8,128)(2,1)S(1)}, bf16[4,48,4096]{2,1,0:T(8,128)(2,1)S(1)}, u32[]{:S(2)}, u32[]{:S(2)}) %collective-permute-start.2) | collective-permute-done | bytes 1572896 | tf_op jit(solution)/shard_map/ppermute | solution.py:19
  200.2 21.6 %collective-permute-done.3 = bf16[4,48,4096]{2,1,0:T(8,128)(2,1)S(1)} collective-permute-done((bf16[4,48,4096]{2,1,0:T(8,128)(2,1)S(1)}, bf16[4,48,4096]{2,1,0:T(8,128)(2,1)S(1)}, u32[]{:S(2)}, u32[]{:S(2)}) %collective-permute-start.3) | collective-permute-done | bytes 1572896 | tf_op jit(solution)/shard_map/ppermute | solution.py:19
  223.0 21.6 %collective-permute-done.4 = bf16[4,48,4096]{2,1,0:T(8,128)(2,1)S(1)} collective-permute-done((bf16[4,48,4096]{2,1,0:T(8,128)(2,1)S(1)}, bf16[4,48,4096]{2,1,0:T(8,128)(2,1)S(1)}, u32[]{:S(2)}, u32[]{:S(2)}) %collective-permute-start.4) | collective-permute-done | bytes 1572896 | tf_op jit(solution)/shard_map/ppermute | solution.py:19
  245.8 21.7 %collective-permute-done.5 = bf16[4,48,4096]{2,1,0:T(8,128)(2,1)} collective-permute-done((bf16[4,48,4096]{2,1,0:T(8,128)(2,1)S(1)}, bf16[4,48,4096]{2,1,0:T(8,128)(2,1)}, u32[]{:S(2)}, u32[]{:S(2)}) %collective-permute-start.5) | collective-permute-done | bytes 1572896 | tf_op jit(solution)/shard_map/ppermute | solution.py:19
  267.6 22.0 %collective-permute-done.6 = bf16[4,48,4096]{2,1,0:T(8,128)(2,1)} collective-permute-done((bf16[4,48,4096]{2,1,0:T(8,128)(2,1)}, bf16[4,48,4096]{2,1,0:T(8,128)(2,1)}, u32[]{:S(2)}, u32[]{:S(2)}) %collective-permute-start.6) | collective-permute-done | bytes 1572896 | tf_op jit(solution)/shard_map/ppermute | solution.py:19
  289.5 2.7 constant_dynamic-update-slice_fusion.15
  292.2 2.8 constant_dynamic-update-slice_fusion.14
  301.0 1.3 constant_dynamic-update-slice_fusion.10
  306.2 2.8 constant_dynamic-update-slice_fusion.7
  308.9 2.7 constant_dynamic-update-slice_fusion.6
  316.7 1.3 constant_dynamic-update-slice_fusion.1
  320.2 7.6 %fusion.30 = f32[32,48,256]{2,1,0:T(8,128)} fusion(bf16[64,48,4096]{2,1,0:T(8,128)(2,1)} %constant_dynamic-update-slice_fusion, s32[]{:T(128)S(6)} %select_n.112, bf16[1,4096,256]{2,1,0:T(8,128)(2,1)S(1)} %copy-done.16), kind=kOutput, calls=%fused_computation.54 | convolution fusion | flops 3221225472 | bytes 16252932 | tf_op jit(solution)/shard_map/rcd,df->rcf/dot_general | solution.py:209
  327.8 19.6 %convolution_convert_fusion = bf16[32,48,4096]{2,1,0:T(8,128)(2,1)} fusion(bf16[1,256,4096]{2,1,0:T(8,128)(2,1)S(1)} %copy-done, f32[32,48,256]{2,1,0:T(8,128)} %fusion.30, bf16[64,48,4096]{2,1,0:T(8,128)(2,1)} %constant_dynamic-update-slice_fusion, s32[]{:T(128)S(6)} %select_n.112, bf16[1,4096,256]{2,1,0:T(8,128)(2,1)} %param.33), kind=kOutput, calls=%fused_computation.58 | convolution fusion | flops 6451101696 | bytes 30932996 | tf_op jit(solution)/shard_map/rcf,fd->rcd/dot_general | solution.py:212
  347.4 126.0 %reduce-scatter.5.cloned.1.call-done = bf16[4,48,4096]{2,1,0:T(8,128)(2,1)} async-done(((bf16[32,48,4096]{2,1,0:T(8,128)(2,1)}), bf16[4,48,4096]{2,1,0:T(8,128)(2,1)}) %reduce-scatter.5.cloned.1.call-update) | async-done | bytes 1572880 | tf_op jit(solution)/shard_map/reduce_scatter | solution.py:211
  473.3 4.6 all-to-all-start.1
  479.0 16.4 %all-to-all-done.1 = bf16[4,48,4096]{2,1,0:T(8,128)(2,1)} async-done(((bf16[4,48,4096]{2,1,0:T(8,128)(2,1)}), bf16[4,48,4096]{2,1,0:T(8,128)(2,1)}, u32[]{:S(2)}, u32[]{:S(2)}) %all-to-all-start.1) | async-done | bytes 1572896 | tf_op jit(solution)/shard_map/all_to_all | solution.py:219
  495.4 3.4 gather_fusion.1
  498.8 2.1 reshape.291
  500.9 3.6 multiply_reduce_fusion
  (166 shorter events, 56.3 us)
Async XLA Ops:
  6.5 321.2 %copy-start = (bf16[1,256,4096]{2,1,0:T(8,128)(2,1)S(1)}, bf16[1,256,4096]{2,1,0:T(8,128)(2,1)}, u32[]{:S(2)}) copy-start(bf16[1,256,4096]{2,1,0:T(8,128)(2,1)} %param.35) | copy-start | bytes 6291460
  6.5 97.3 %reduce-scatter.3.cloned.1.call-start = ((), (), s32[]{:S(2)}) async-start(), calls=%async_computation.4 | async-start | bytes 3538944 | tf_op jit(solution)/shard_map/reduce_scatter | solution.py:192
  44.1 12.9 %copy-start.15 = (f32[256]{0:T(256)S(1)}, f32[256]{0:T(256)}, u32[]{:S(2)}) copy-start(f32[256]{0:T(256)} %param.27) | copy-start | bytes 3076
  55.8 2.6 copy-start.13
  63.0 42.2 %copy-start.14 = (f32[4096]{0:T(1024)S(1)}, f32[4096]{0:T(1024)}, u32[]{:S(2)}) copy-start(f32[4096]{0:T(1024)} %param.30) | copy-start | bytes 49156
  63.0 410.3 %reduce-scatter.5.cloned.1.call-start = ((), (), s32[]{:S(2)}) async-start(), calls=%async_computation.5 | async-start | bytes 14155776 | tf_op jit(solution)/shard_map/reduce_scatter | solution.py:211
  130.7 1.1 copy-start.1
  131.8 21.6 %collective-permute-start = (bf16[4,48,4096]{2,1,0:T(8,128)(2,1)S(1)}, bf16[4,48,4096]{2,1,0:T(8,128)(2,1)S(1)}, u32[]{:S(2)}, u32[]{:S(2)}) collective-permute-start(bf16[4,48,4096]{2,1,0:T(8,128)(2,1)S(1)} %all_to_all.10), channel_id=1, source_target_pairs={{0,1},{1,2},{2,3},{3,4},{4,5},{5,6},{6,7},{7,0},{8,9},{9,10},{10,1... | collective-permute-start | bytes 4718600 | tf_op jit(solution)/shard_map/ppermute | solution.py:19
  153.4 1.2 copy-start.3
  154.6 21.6 %collective-permute-start.1 = (bf16[4,48,4096]{2,1,0:T(8,128)(2,1)S(1)}, bf16[4,48,4096]{2,1,0:T(8,128)(2,1)S(1)}, u32[]{:S(2)}, u32[]{:S(2)}) collective-permute-start(bf16[4,48,4096]{2,1,0:T(8,128)(2,1)S(1)} %collective-permute-done), channel_id=1, source_target_pairs={{0,1},{1,2},{2,3},{3,4},{4,5},{5,6},{6,7},{7,0},{8,9},{9,10},{10,1... | collective-permute-start | bytes 4718600 | tf_op jit(solution)/shard_map/ppermute | solution.py:19
  176.2 1.2 copy-start.5
  177.4 21.6 %collective-permute-start.2 = (bf16[4,48,4096]{2,1,0:T(8,128)(2,1)S(1)}, bf16[4,48,4096]{2,1,0:T(8,128)(2,1)S(1)}, u32[]{:S(2)}, u32[]{:S(2)}) collective-permute-start(bf16[4,48,4096]{2,1,0:T(8,128)(2,1)S(1)} %collective-permute-done.1), channel_id=1, source_target_pairs={{0,1},{1,2},{2,3},{3,4},{4,5},{5,6},{6,7},{7,0},{8,9},{9,10},{10,1... | collective-permute-start | bytes 4718600 | tf_op jit(solution)/shard_map/ppermute | solution.py:19
  199.1 1.1 copy-start.7
  200.2 21.6 %collective-permute-start.3 = (bf16[4,48,4096]{2,1,0:T(8,128)(2,1)S(1)}, bf16[4,48,4096]{2,1,0:T(8,128)(2,1)S(1)}, u32[]{:S(2)}, u32[]{:S(2)}) collective-permute-start(bf16[4,48,4096]{2,1,0:T(8,128)(2,1)S(1)} %collective-permute-done.2), channel_id=1, source_target_pairs={{0,1},{1,2},{2,3},{3,4},{4,5},{5,6},{6,7},{7,0},{8,9},{9,10},{10,1... | collective-permute-start | bytes 4718600 | tf_op jit(solution)/shard_map/ppermute | solution.py:19
  221.8 1.1 copy-start.9
  223.0 21.6 %collective-permute-start.4 = (bf16[4,48,4096]{2,1,0:T(8,128)(2,1)S(1)}, bf16[4,48,4096]{2,1,0:T(8,128)(2,1)S(1)}, u32[]{:S(2)}, u32[]{:S(2)}) collective-permute-start(bf16[4,48,4096]{2,1,0:T(8,128)(2,1)S(1)} %collective-permute-done.3), channel_id=1, source_target_pairs={{0,1},{1,2},{2,3},{3,4},{4,5},{5,6},{6,7},{7,0},{8,9},{9,10},{10,1... | collective-permute-start | bytes 4718600 | tf_op jit(solution)/shard_map/ppermute | solution.py:19
  244.6 1.2 copy-start.11
  245.8 21.7 %collective-permute-start.5 = (bf16[4,48,4096]{2,1,0:T(8,128)(2,1)S(1)}, bf16[4,48,4096]{2,1,0:T(8,128)(2,1)}, u32[]{:S(2)}, u32[]{:S(2)}) collective-permute-start(bf16[4,48,4096]{2,1,0:T(8,128)(2,1)S(1)} %collective-permute-done.4), channel_id=1, source_target_pairs={{0,1},{1,2},{2,3},{3,4},{4,5},{5,6},{6,7},{7,0},{8,9},{9,10},{10,1... | collective-permute-start | bytes 4718600 | tf_op jit(solution)/shard_map/ppermute | solution.py:19
  267.6 22.0 %collective-permute-start.6 = (bf16[4,48,4096]{2,1,0:T(8,128)(2,1)}, bf16[4,48,4096]{2,1,0:T(8,128)(2,1)}, u32[]{:S(2)}, u32[]{:S(2)}) collective-permute-start(bf16[4,48,4096]{2,1,0:T(8,128)(2,1)} %collective-permute-done.5), channel_id=1, source_target_pairs={{0,1},{1,2},{2,3},{3,4},{4,5},{5,6},{6,7},{7,0},{8,9},{9,10},{10,1... | collective-permute-start | bytes 4718600 | tf_op jit(solution)/shard_map/ppermute | solution.py:19
  292.2 2.8 copy-start.12
  295.1 2.0 copy-start.10
  297.0 2.0 copy-start.8
  299.0 2.0 copy-start.6
  301.0 2.0 copy-start.4
  303.0 2.0 copy-start.2
  318.0 2.2 copy-start.16
  473.3 22.1 %all-to-all-start.1 = ((bf16[4,48,4096]{2,1,0:T(8,128)(2,1)}), bf16[4,48,4096]{2,1,0:T(8,128)(2,1)}, u32[]{:S(2)}, u32[]{:S(2)}) async-start(bf16[4,48,4096]{2,1,0:T(8,128)(2,1)} %reduce-scatter.5.cloned.1.call-done), calls=%async_computation.3 | async-start | bytes 3145728 | tf_op jit(solution)/shard_map/all_to_all | solution.py:219
Sparse Core Ops, SparseCore 0:
  63.1 40.6 reduce-scatter.2
  347.5 125.8 reduce-scatter.4
